TPU v7x, 32 devices: a whole 2x2x4 slice. The times are simulated.
32 devices in a mesh: sp: 8 (over z, x), dp: 4 (over y, core).
Axes of the slice: x: 2, y: 2, z: 4, core: 2. Of those that a mesh axis runs over, the one named last changes fastest.
Arguments:
- queries: bfloat16 [16, 8, 512, 256], P('dp', None, 'sp'), may hold values from -6 to 6
- keys: bfloat16 [16, 8, 512, 256], P('dp', None, 'sp'), may hold values from -6 to 6
- values: bfloat16 [16, 8, 512, 256], P('dp', None, 'sp'), may hold values from -6 to 6
- log_decay: float32 [128, 512], P(('dp', 'sp')), may hold values from -2 to 0, as said below
- w_out: bfloat16 [8, 256, 2048], P(None, None, 'dp'), may hold values from -0.125 to 0.125
Outputs:
- mixed_out: bfloat16 [16, 512, 2048], P('dp', 'sp')
Inputs may be any that keep to these rules, and one draw needn't show every extreme that they name: Every entry of log_decay is below zero.
All inputs are finite; a program needn't handle non-finite values.
Results may differ from a plain program's by a relative error of at most 0.008.
Values may be sent and summed in bfloat16 or wider, within the bound.
A program may use at most 128 MiB of HBM per device.

v0:
```python
import jax
import jax.numpy as jnp
from jax import lax
from jax.sharding import PartitionSpec as P

BLOCK = 64


def rotate(field_in, cosine, sine_tab):
    half_dim = field_in.shape[1] // 2
    widened = field_in.astype(jnp.float32)
    first_half = widened[:, :half_dim]
    second_half = widened[:, half_dim:]
    turned = jnp.concatenate(
        [
            first_half * cosine - second_half * sine_tab,
            second_half * cosine + first_half * sine_tab,
        ],
        axis=1,
    )
    return turned.astype(jnp.bfloat16)


def retain(query_rows, key_rows, value_rows, decay_row, cosine, sine_tab):
    length, head_width = query_rows.shape
    blocks = length // BLOCK
    rot_query = rotate(query_rows, cosine, sine_tab).reshape(blocks, BLOCK, head_width)
    rot_key = rotate(key_rows, cosine, sine_tab).reshape(blocks, BLOCK, head_width)
    value_blocks = value_rows.reshape(blocks, BLOCK, head_width)
    within = jnp.cumsum(decay_row.reshape(blocks, BLOCK), axis=1)
    ending = within[:, -1:]
    causal = jnp.tril(jnp.ones((BLOCK, BLOCK), dtype=bool))[None]
    spread = within[:, :, None] - within[:, None, :]
    decay_mask = jnp.where(causal, jnp.exp(jnp.where(causal, spread, 0.0)), 0.0)
    scores = jnp.einsum("bnd,bmd->bnm", rot_query, rot_key, preferred_element_type=jnp.float32)
    weights = (scores * decay_mask).astype(jnp.bfloat16)
    scaled_keys = (rot_key * jnp.exp(ending - within)[:, :, None]).astype(jnp.bfloat16)
    updates = jnp.einsum(
        "bmd,bme->bde", scaled_keys, value_blocks, preferred_element_type=jnp.float32
    )

    def advance(state_now, inputs):
        factor, update = inputs
        return (factor * state_now + update, state_now.astype(jnp.bfloat16))

    start_state = jnp.zeros((head_width, head_width), jnp.float32)
    _, before = lax.scan(advance, start_state, (jnp.exp(ending[:, 0]), updates))
    local_part = jnp.einsum(
        "bnm,bme->bne", weights, value_blocks, preferred_element_type=jnp.float32
    )
    carried = jnp.einsum("bnd,bde->bne", rot_query, before, preferred_element_type=jnp.float32)
    combined = local_part + jnp.exp(within)[:, :, None] * carried
    return combined.reshape(length, head_width).astype(jnp.bfloat16)


def on_device(queries, keys, values, log_decay, w_out):
    groups, head_count, seg_len, head_width = queries.shape
    item_count = groups * head_count
    flat_q = queries.reshape(item_count, seg_len, head_width)
    flat_k = keys.reshape(item_count, seg_len, head_width)
    flat_v = values.reshape(item_count, seg_len, head_width)
    head_k, head_v = (
        lax.all_to_all(flat_k, "sp", split_axis=0, concat_axis=1, tiled=True),
        lax.all_to_all(flat_v, "sp", split_axis=0, concat_axis=1, tiled=True),
    )
    head_q = lax.all_to_all(flat_q, "sp", split_axis=0, concat_axis=1, tiled=True)
    length = head_q.shape[1]
    half_dim = head_width // 2
    frequency = 10000.0 ** (-jnp.arange(half_dim, dtype=jnp.float32) / half_dim)
    angles = jnp.arange(length, dtype=jnp.float32)[:, None] * frequency[None, :]
    cosine = jnp.cos(angles)
    sine_tab = jnp.sin(angles)

    def one_item(inputs):
        return retain(inputs[0], inputs[1], inputs[2], inputs[3], cosine, sine_tab)

    retained = lax.map(one_item, (head_q, head_k, head_v, log_decay))
    by_token = lax.all_to_all(retained, "sp", split_axis=1, concat_axis=0, tiled=True)
    by_token = by_token.reshape(groups, head_count, seg_len, head_width)
    widened = by_token.astype(jnp.float32)
    normed = (
        widened * lax.rsqrt(jnp.mean(widened * widened, axis=-1, keepdims=True) + 1e-06)
    ).astype(jnp.bfloat16)
    mixed_out = jnp.einsum(
        "shtd,hde->ste",
        normed,
        lax.all_gather(w_out, "dp", axis=2, tiled=True),
        preferred_element_type=jnp.float32,
    )
    return mixed_out.astype(jnp.bfloat16)


def solution(mesh):
    placed = (
        P("dp", None, "sp", None),
        P("dp", None, "sp", None),
        P("dp", None, "sp", None),
        P(("dp", "sp"), None),
        P(None, None, "dp"),
    )
    return jax.shard_map(
        on_device, mesh=mesh, in_specs=placed, out_specs=P("dp", "sp", None), check_vma=False
    )
```

profile of v0, /device:TPU:0, one launch (start us, length us, event | category | flops | bytes accessed | tf_op | source)
XLA Modules:
  0.0 242.2 jit_solution(14307589264207442078)
XLA Ops:
  6.5 33.2 %all_to_all.63 = bf16[32,64,256]{2,1,0:T(8,128)(2,1)S(1)} all-to-all(bf16[32,64,256]{2,1,0:T(8,128)(2,1)} %bitcast.108), channel_id=1, replica_groups=mesh['sp'=8,'dp'=4] {'sp'}, dimensions={0} | all-to-all | bytes 2097152 | tf_op jit(solution)/shard_map/all_to_all | solution.py:64
  39.7 28.8 %all_to_all.64 = bf16[32,64,256]{2,1,0:T(8,128)(2,1)S(1)} all-to-all(bf16[32,64,256]{2,1,0:T(8,128)(2,1)S(1)} %bitcast.109), channel_id=1, replica_groups=mesh['sp'=8,'dp'=4] {'sp'}, dimensions={0} | all-to-all | bytes 2097152 | tf_op jit(solution)/shard_map/all_to_all | solution.py:66
  68.6 3.6 %all-to-all-start.1 = ((bf16[32,64,256]{2,1,0:T(8,128)(2,1)}), bf16[32,64,256]{2,1,0:T(8,128)(2,1)S(1)}, u32[]{:S(2)}, u32[]{:S(2)}) async-start(bf16[32,64,256]{2,1,0:T(8,128)(2,1)} %bitcast.110), calls=%async_computation.1 | async-start | bytes 2097152 | tf_op jit(solution)/shard_map/all_to_all | solution.py:63
  72.9 1.0 copy.28
  73.9 1.1 copy.26
  75.1 22.6 %all-to-all-done.1 = bf16[32,64,256]{2,1,0:T(8,128)(2,1)S(1)} async-done(((bf16[32,64,256]{2,1,0:T(8,128)(2,1)}), bf16[32,64,256]{2,1,0:T(8,128)(2,1)S(1)}, u32[]{:S(2)}, u32[]{:S(2)}) %all-to-all-start.1) | async-done | bytes 1048608 | tf_op jit(solution)/shard_map/all_to_all | solution.py:63
  97.6 1.0 copy.27
  98.7 97.2 %while.30 = (s32[]{:T(128)}, bf16[4,512,256]{2,1,0:T(8,128)(2,1)}, bf16[4,512,256]{2,1,0:T(8,128)(2,1)}, bf16[4,512,256]{2,1,0:T(8,128)(2,1)}, f32[4,512]{1,0:T(...) while((s32[]{:T(128)}, bf16[4,512,256]{2,1,0:T(8,128)(2,1)}, ...), condition=%wide.region_4.5_spmd.clone.clone.clone, body=%wide.region_0.4_spmd.clone.clone.clone.sunk | while | flops 172363776 | bytes 15632365 | solution.py:77
  98.7 1.1 bitcast_convert_fusion.3
  99.8 1.2 fusion.70
  102.2 1.0 constant_dynamic-slice_fusion.2
  103.2 0.7 fusion.73
  104.0 16.7 %while.31 = (s32[]{:T(128)}, f32[256,256]{1,0:T(8,128)S(1)}, bf16[8,256,256]{2,1,0:T(8,128)(2,1)}, f32[8]{0:T(128)S(1)}, f32[8,256,256]{2,1,0:T(8,128)S(1)}, /*index=5*/s32[]{:T(128)}, s32[]{:T(128)}) while((s32[]{:T(128)}, f32[256,256]{1,0:T(8,128)S(1)}, bf16[8,256,256]{2,1,0:T(8,128)(2,1)}, f32[8]{0:T(128)S(1)}, ...), condition=%wide.region_3.3_spmd.clone, body=%wide.region_2.2_spmd.clone.sunk | while | flops 262147 | bytes 1180268 | solution.py:47
  105.3 0.8 bitcast_add_fusion.2
  107.4 0.8 bitcast_add_fusion.2
  109.5 0.8 bitcast_add_fusion.2
  111.6 0.8 bitcast_add_fusion.2
  113.7 0.8 bitcast_add_fusion.2
  115.8 0.8 bitcast_add_fusion.2
  117.9 0.8 bitcast_add_fusion.2
  120.0 0.8 bitcast_add_fusion.2
  121.1 0.9 copy-done
  123.0 1.1 bitcast_convert_fusion.3
  124.1 1.2 fusion.70
  126.6 1.0 constant_dynamic-slice_fusion.2
  128.3 16.7 %while.31 = (s32[]{:T(128)}, f32[256,256]{1,0:T(8,128)S(1)}, bf16[8,256,256]{2,1,0:T(8,128)(2,1)}, f32[8]{0:T(128)S(1)}, f32[8,256,256]{2,1,0:T(8,128)S(1)}, /*index=5*/s32[]{:T(128)}, s32[]{:T(128)}) while((s32[]{:T(128)}, f32[256,256]{1,0:T(8,128)S(1)}, bf16[8,256,256]{2,1,0:T(8,128)(2,1)}, f32[8]{0:T(128)S(1)}, ...), condition=%wide.region_3.3_spmd.clone, body=%wide.region_2.2_spmd.clone.sunk | while | flops 262147 | bytes 1180268 | solution.py:47
  129.6 0.8 bitcast_add_fusion.2
  131.7 0.8 bitcast_add_fusion.2
  133.8 0.8 bitcast_add_fusion.2
  135.9 0.8 bitcast_add_fusion.2
  138.0 0.8 bitcast_add_fusion.2
  140.1 0.8 bitcast_add_fusion.2
  142.2 0.8 bitcast_add_fusion.2
  144.3 0.8 bitcast_add_fusion.2
  145.4 0.9 copy-done
  147.3 1.1 bitcast_convert_fusion.3
  148.4 1.2 fusion.70
  150.9 1.0 constant_dynamic-slice_fusion.2
  152.6 16.7 %while.31 = (s32[]{:T(128)}, f32[256,256]{1,0:T(8,128)S(1)}, bf16[8,256,256]{2,1,0:T(8,128)(2,1)}, f32[8]{0:T(128)S(1)}, f32[8,256,256]{2,1,0:T(8,128)S(1)}, /*index=5*/s32[]{:T(128)}, s32[]{:T(128)}) while((s32[]{:T(128)}, f32[256,256]{1,0:T(8,128)S(1)}, bf16[8,256,256]{2,1,0:T(8,128)(2,1)}, f32[8]{0:T(128)S(1)}, ...), condition=%wide.region_3.3_spmd.clone, body=%wide.region_2.2_spmd.clone.sunk | while | flops 262147 | bytes 1180268 | solution.py:47
  154.0 0.8 bitcast_add_fusion.2
  156.0 0.8 bitcast_add_fusion.2
  158.1 0.8 bitcast_add_fusion.2
  160.2 0.8 bitcast_add_fusion.2
  162.3 0.8 bitcast_add_fusion.2
  164.4 0.8 bitcast_add_fusion.2
  166.5 0.8 bitcast_add_fusion.2
  168.6 0.8 bitcast_add_fusion.2
  169.7 0.9 copy-done
  171.6 1.1 bitcast_convert_fusion.3
  172.7 1.2 fusion.70
  175.2 1.0 constant_dynamic-slice_fusion.2
  176.9 16.7 %while.31 = (s32[]{:T(128)}, f32[256,256]{1,0:T(8,128)S(1)}, bf16[8,256,256]{2,1,0:T(8,128)(2,1)}, f32[8]{0:T(128)S(1)}, f32[8,256,256]{2,1,0:T(8,128)S(1)}, /*index=5*/s32[]{:T(128)}, s32[]{:T(128)}) while((s32[]{:T(128)}, f32[256,256]{1,0:T(8,128)S(1)}, bf16[8,256,256]{2,1,0:T(8,128)(2,1)}, f32[8]{0:T(128)S(1)}, ...), condition=%wide.region_3.3_spmd.clone, body=%wide.region_2.2_spmd.clone.sunk | while | flops 262147 | bytes 1180268 | solution.py:47
  178.3 0.8 bitcast_add_fusion.2
  180.4 0.8 bitcast_add_fusion.2
  182.4 0.8 bitcast_add_fusion.2
  184.5 0.8 bitcast_add_fusion.2
  186.6 0.8 bitcast_add_fusion.2
  188.7 0.8 bitcast_add_fusion.2
  190.8 0.8 bitcast_add_fusion.2
  192.9 0.8 bitcast_add_fusion.2
  194.0 0.9 copy-done
  195.9 2.0 copy.29
  198.0 29.1 %all_to_all.65 = bf16[4,512,256]{2,0,1:T(4,128)(2,1)S(1)} all-to-all(bf16[4,512,256]{2,0,1:T(4,128)(2,1)S(1)} %copy.29), channel_id=1, replica_groups=mesh['sp'=8,'dp'=4] {'sp'}, dimensions={1} | all-to-all | bytes 2097152 | tf_op jit(solution)/shard_map/all_to_all | solution.py:78
  228.5 6.8 %fusion.48 = bf16[4,64,2048]{2,1,0:T(8,128)(2,1)} fusion(bf16[8,256,2048]{2,1,0:T(8,128)(2,1)} %all-gather.2.cloned.1.call-done, f32[4,8,64]{2,1,0:T(8,128)S(1)} %bitcast.112, f32[4,8,64,256]{3,2,1,0:T(8,128)S(1)} %bitcast.107), kind=kOutput, calls=%fused_computation.59 | convolution fusion | flops 2149056512 | bytes 11542528 | tf_op jit(solution)/shard_map/shtd,hde->ste/dot_general | solution.py:84
  (131 shorter events, 57.3 us)
Async XLA Ops:
  6.5 33.2 %copy-start.1 = (bf16[4,8,64,256]{3,2,1,0:T(8,128)(2,1)S(1)}, bf16[4,8,64,256]{3,2,1,0:T(8,128)(2,1)}, u32[]{:S(2)}) copy-start(bf16[4,8,64,256]{3,2,1,0:T(8,128)(2,1)} %param.9) | copy-start | bytes 3145732
  68.6 29.1 %all-to-all-start.1 = ((bf16[32,64,256]{2,1,0:T(8,128)(2,1)}), bf16[32,64,256]{2,1,0:T(8,128)(2,1)S(1)}, u32[]{:S(2)}, u32[]{:S(2)}) async-start(bf16[32,64,256]{2,1,0:T(8,128)(2,1)} %bitcast.110), calls=%async_computation.1 | async-start | bytes 2097152 | tf_op jit(solution)/shard_map/all_to_all | solution.py:63
  72.1 156.4 %all-gather.2.cloned.1.call-start = ((), (), s32[]{:S(2)}) async-start(), calls=%async_computation.4 | async-start | bytes 10485760 | tf_op jit(solution)/shard_map/all_gather | solution.py:87
  120.7 1.2 copy-start
  145.0 1.2 copy-start
  169.3 1.2 copy-start
  193.7 1.2 copy-start
Sparse Core Ops, SparseCore 0:
  74.5 59.6 all-gather.1
where the time goes:
time: 243 us; the launch traced here: 242 us
  blocking collectives  91.1 us (37%)
  other arithmetic  56.7 us (23%)
  local copies, waits for them, and re-layouts  40.7 us (17%)
  waiting for transfers between devices  23.3 us (10%)
  between operations  13.5 us (6%)
  matrix products  12.3 us (5%)
  starting transfers between devices  3.6 us (1%)
    all_to_all x1, blocking collectives, on_device(): lax.all_to_all(flat_v, 'sp', split_axis=0, concat_axis=1, tiled=True)  33.2 us
    all_to_all x1, blocking collectives, on_device(): lax.all_to_all(retained, 'sp', split_axis=1, concat_axis=0, tiled=True)  29.1 us
    all_to_all x1, blocking collectives, on_device(): lax.all_to_all(flat_q, 'sp', split_axis=0, concat_axis=1, tiled=True)  28.8 us
    add x32, other arithmetic, advance(): return (factor * state_now + update, state_now.astype(jnp.bfloat16))  24 us
    all_to_all x1, waiting for transfers between devices, on_device(): lax.all_to_all(flat_k, 'sp', split_axis=0, concat_axis=1, tiled=True)  22.6 us
    dynamic_update_slice x32, other arithmetic, retain(): _, before = lax.scan(advance, start_state, (jnp.exp(ending[:, 0]), updates))  21.5 us
    dynamic_slice x32, local copies, waits for them, and re-layouts, retain(): _, before = lax.scan(advance, start_state, (jnp.exp(ending[:, 0]), updates))  20.7 us
    dynamic_slice x8, local copies, waits for them, and re-layouts, on_device(): retained = lax.map(one_item, (head_q, head_k, head_v, log_decay))  6.8 us
  transfers between devices with their start and end apart: 2, of which 1 were waited for; matrix products, arithmetic and copies ran while one was open for 41% of the time, Pallas kernels for 0%

commit v1 on v0

--- a/solution.py
+++ b/solution.py
@@ -4,6 +4,29 @@
 from jax.sharding import PartitionSpec as P
 
 BLOCK = 64
+
+
+def cut_along(x, dim, peers):
+    dims = x.shape
+    parts = x.reshape(*dims[:dim], peers, dims[dim] // peers, *dims[dim + 1 :])
+    return jnp.moveaxis(parts, dim, 0)
+
+
+def joined_along(blocks, dim):
+    lengths = list(blocks.shape[1:])
+    lengths[dim] *= blocks.shape[0]
+    return jnp.moveaxis(blocks, 0, dim).reshape(lengths)
+
+
+def swapped_with_each(x, axis, split_dim, concat_dim):
+    size, place = (lax.axis_size(axis), lax.axis_index(axis))
+    blocks = cut_along(x, split_dim, size)
+    outs = [blocks[place]]
+    for step in range(1, size):
+        sent = blocks[place ^ step]
+        outs.append(lax.ppermute(sent, axis, [(i, i ^ step) for i in range(size)]))
+    blocks = jnp.stack(outs)[place ^ jnp.arange(size)]
+    return joined_along(blocks, concat_dim)
 
 
 def rotate(field_in, cosine, sine_tab):
@@ -61,7 +84,7 @@
     flat_v = values.reshape(item_count, seg_len, head_width)
     head_k, head_v = (
         lax.all_to_all(flat_k, "sp", split_axis=0, concat_axis=1, tiled=True),
-        lax.all_to_all(flat_v, "sp", split_axis=0, concat_axis=1, tiled=True),
+        swapped_with_each(flat_v, "sp", 0, 1),
     )
     head_q = lax.all_to_all(flat_q, "sp", split_axis=0, concat_axis=1, tiled=True)
     length = head_q.shape[1]

time: 243 us -> 231 us (0.951)
  blocking collectives: 91.1 us -> 37.4 us
  starting transfers between devices: 3.6 us -> 24 us
  waiting for transfers between devices: 23.3 us -> 39.4 us
  local copies, waits for them, and re-layouts: 40.7 us -> 46.9 us
    all_to_all x2 -> x0, blocking collectives: 62 us -> none  [the longest x1 33.2 us: on_device(): lax.all_to_all(flat_v, 'sp', split_axis=0, concat_axis=1, tiled=True)]
    all_to_all x0 -> x1, waiting for transfers between devices: none -> 24 us  [on_device(): lax.all_to_all(flat_q, 'sp', split_axis=0, concat_axis=1, tiled=True)]
    all_to_all x1, waiting for transfers between devices: 22.6 us -> 3.22 us  [on_device(): lax.all_to_all(flat_k, 'sp', split_axis=0, concat_axis=1, tiled=True)]
    ppermute x0 -> x7, starting transfers between devices: none -> 13 us  [swapped_with_each(): outs.append(lax.ppermute(sent, axis, [(i, i ^ step) for i in range(size)]))]
    ppermute x0 -> x7, waiting for transfers between devices: none -> 12.1 us  [swapped_with_each(): outs.append(lax.ppermute(sent, axis, [(i, i ^ step) for i in range(size)]))]
    all_to_all x1, blocking collectives: 29.1 us -> 37.4 us  [on_device(): lax.all_to_all(retained, 'sp', split_axis=1, concat_axis=0, tiled=True)]
    all_to_all x0 -> x1, starting transfers between devices: none -> 7.41 us  [on_device(): lax.all_to_all(flat_q, 'sp', split_axis=0, concat_axis=1, tiled=True)]
    unnamed x2 -> x8, local copies, waits for them, and re-layouts: 0.01 us -> 4.88 us
  transfers between devices with their start and end apart: 2 -> 10, of which waited for: 1 -> 5; matrix products, arithmetic and copies ran while one was open for 41% -> 45% of each run, Pallas kernels for 0% -> 0%
where the time goes in v1:
time: 231 us; the launch traced here: 229 us
  other arithmetic  54.9 us (24%)
  local copies, waits for them, and re-layouts  46.9 us (20%)
  waiting for transfers between devices  39.4 us (17%)
  blocking collectives  37.4 us (16%)
  starting transfers between devices  24 us (10%)
  between operations  13.5 us (6%)
  matrix products  12.2 us (5%)
    all_to_all x1, blocking collectives, on_device(): lax.all_to_all(retained, 'sp', split_axis=1, concat_axis=0, tiled=True)  37.4 us
    all_to_all x1, waiting for transfers between devices, on_device(): lax.all_to_all(flat_q, 'sp', split_axis=0, concat_axis=1, tiled=True)  24 us
    add x32, other arithmetic, advance(): return (factor * state_now + update, state_now.astype(jnp.bfloat16))  22.1 us
    dynamic_update_slice x32, other arithmetic, retain(): _, before = lax.scan(advance, start_state, (jnp.exp(ending[:, 0]), updates))  21.5 us
    dynamic_slice x32, local copies, waits for them, and re-layouts, retain(): _, before = lax.scan(advance, start_state, (jnp.exp(ending[:, 0]), updates))  18.8 us
    ppermute x7, starting transfers between devices, swapped_with_each(): outs.append(lax.ppermute(sent, axis, [(i, i ^ step) for i in range(size)]))  13 us
    ppermute x7, waiting for transfers between devices, swapped_with_each(): outs.append(lax.ppermute(sent, axis, [(i, i ^ step) for i in range(size)]))  12.1 us
    all_to_all x1, starting transfers between devices, on_device(): lax.all_to_all(flat_q, 'sp', split_axis=0, concat_axis=1, tiled=True)  7.41 us
  transfers between devices with their start and end apart: 10, of which 5 were waited for; matrix products, arithmetic and copies ran while one was open for 45% of the time, Pallas kernels for 0%

profile of v1, /device:TPU:0, one launch (start us, length us, event | category | flops | bytes accessed | tf_op | source)
XLA Modules:
  0.0 229.4 jit_solution(11022641974284253689)
XLA Ops:
  6.5 7.4 %all-to-all-start = ((bf16[32,64,256]{2,1,0:T(8,128)(2,1)}), bf16[32,64,256]{2,1,0:T(8,128)(2,1)S(1)}, u32[]{:S(2)}, u32[]{:S(2)}) async-start(bf16[32,64,256]{2,1,0:T(8,128)(2,1)} %bitcast.137), calls=%async_computation | async-start | bytes 2097152 | tf_op jit(solution)/shard_map/all_to_all | solution.py:89
  14.0 0.8 dynamic-slice_bitcast_fusion
  14.8 1.9 collective-permute-start
  16.8 1.5 collective-permute-start.1
  18.3 2.8 %collective-permute-start.3 = (bf16[4,64,256]{2,1,0:T(8,128)(2,1)S(1)}, bf16[4,64,256]{2,1,0:T(8,128)(2,1)S(1)}, u32[]{:S(2)}, u32[]{:S(2)}) collective-permute-start(bf16[4,64,256]{2,1,0:T(8,128)(2,1)S(1)} %get-tuple-element.223), channel_id=1, source_target_pairs={{0,16},{4,20},{8,24},{12,28},{16,0},{20,4},{24,8},{28,12},{1,17},{... | collective-permute-start | bytes 393224 | tf_op jit(solution)/shard_map/ppermute | solution.py:27
  21.2 1.5 collective-permute-start.4
  22.7 24.0 %all-to-all-done = bf16[32,64,256]{2,1,0:T(8,128)(2,1)S(1)} async-done(((bf16[32,64,256]{2,1,0:T(8,128)(2,1)}), bf16[32,64,256]{2,1,0:T(8,128)(2,1)S(1)}, u32[]{:S(2)}, u32[]{:S(2)}) %all-to-all-start) | async-done | bytes 1048608 | tf_op jit(solution)/shard_map/all_to_all | solution.py:89
  46.7 3.6 %all-to-all-start.1 = ((bf16[32,64,256]{2,1,0:T(8,128)(2,1)}), bf16[32,64,256]{2,1,0:T(8,128)(2,1)S(1)}, u32[]{:S(2)}, u32[]{:S(2)}) async-start(bf16[32,64,256]{2,1,0:T(8,128)(2,1)} %bitcast.4), calls=%async_computation.1 | async-start | bytes 2097152 | tf_op jit(solution)/shard_map/all_to_all | solution.py:86
  50.3 3.8 %collective-permute-start.5 = (bf16[4,64,256]{2,1,0:T(8,128)(2,1)S(1)}, bf16[4,64,256]{2,1,0:T(8,128)(2,1)S(1)}, u32[]{:S(2)}, u32[]{:S(2)}) collective-permute-start(bf16[4,64,256]{2,1,0:T(8,128)(2,1)S(1)} %get-tuple-element.221), channel_id=1, source_target_pairs={{0,24},{4,28},{8,16},{12,20},{16,8},{20,12},{24,0},{28,4},{1,25},{... | collective-permute-start | bytes 393224 | tf_op jit(solution)/shard_map/ppermute | solution.py:27
  54.1 1.6 bitcast_dynamic-update-slice_fusion.7
  55.7 1.4 collective-permute-start.6
  60.5 9.7 %collective-permute-done.5 = bf16[4,64,256]{2,1,0:T(8,128)(2,1)S(1)} collective-permute-done((bf16[4,64,256]{2,1,0:T(8,128)(2,1)S(1)}, bf16[4,64,256]{2,1,0:T(8,128)(2,1)S(1)}, u32[]{:S(2)}, u32[]{:S(2)}) %collective-permute-start.5) | collective-permute-done | bytes 131104 | tf_op jit(solution)/shard_map/ppermute | solution.py:27
  70.8 1.8 collective-permute-done.6
  73.2 1.8 gather_fusion
  75.1 1.1 copy.28
  76.1 1.1 copy.26
  77.3 3.2 %all-to-all-done.1 = bf16[32,64,256]{2,1,0:T(8,128)(2,1)S(1)} async-done(((bf16[32,64,256]{2,1,0:T(8,128)(2,1)}), bf16[32,64,256]{2,1,0:T(8,128)(2,1)S(1)}, u32[]{:S(2)}, u32[]{:S(2)}) %all-to-all-start.1) | async-done | bytes 1048608 | tf_op jit(solution)/shard_map/all_to_all | solution.py:86
  80.5 1.0 copy.27
  81.5 93.5 %while.30 = (s32[]{:T(128)}, bf16[4,512,256]{2,1,0:T(8,128)(2,1)}, bf16[4,512,256]{2,1,0:T(8,128)(2,1)}, bf16[4,512,256]{2,1,0:T(8,128)(2,1)}, f32[4,512]{1,0:T(...) while((s32[]{:T(128)}, bf16[4,512,256]{2,1,0:T(8,128)(2,1)}, ...), condition=%wide.region_4.5_spmd.clone.clone.clone, body=%wide.region_0.4_spmd.clone.clone.clone.sunk | while | flops 172363776 | bytes 15632365 | solution.py:100
  81.5 1.1 bitcast_convert_fusion.3
  82.6 1.2 fusion.71
  83.8 0.7 dynamic-slice_reduce_fusion.2
  85.1 1.0 constant_dynamic-slice_fusion.2
  86.1 0.7 fusion.74
  86.8 15.8 %while.31 = (s32[]{:T(128)}, f32[256,256]{1,0:T(8,128)S(1)}, bf16[8,256,256]{2,1,0:T(8,128)(2,1)}, f32[8]{0:T(128)S(1)}, f32[8,256,256]{2,1,0:T(8,128)S(1)}, /*index=5*/s32[]{:T(128)}, s32[]{:T(128)}) while((s32[]{:T(128)}, f32[256,256]{1,0:T(8,128)S(1)}, bf16[8,256,256]{2,1,0:T(8,128)(2,1)}, f32[8]{0:T(128)S(1)}, ...), condition=%wide.region_3.3_spmd.clone, body=%wide.region_2.2_spmd.clone.sunk | while | flops 262147 | bytes 1180268 | solution.py:70
  88.1 0.7 bitcast_add_fusion.2
  90.1 0.7 bitcast_add_fusion.2
  92.1 0.7 bitcast_add_fusion.2
  94.0 0.7 bitcast_add_fusion.2
  96.0 0.7 bitcast_add_fusion.2
  98.0 0.7 bitcast_add_fusion.2
  99.9 0.7 bitcast_add_fusion.2
  103.0 0.9 copy-done
  104.2 0.7 bitcast_dynamic-update-slice_fusion.9
  104.9 1.1 bitcast_convert_fusion.3
  106.0 1.2 fusion.71
  107.2 0.7 dynamic-slice_reduce_fusion.2
  108.5 1.0 constant_dynamic-slice_fusion.2
  109.4 0.7 fusion.74
  110.2 15.8 %while.31 = (s32[]{:T(128)}, f32[256,256]{1,0:T(8,128)S(1)}, bf16[8,256,256]{2,1,0:T(8,128)(2,1)}, f32[8]{0:T(128)S(1)}, f32[8,256,256]{2,1,0:T(8,128)S(1)}, /*index=5*/s32[]{:T(128)}, s32[]{:T(128)}) while((s32[]{:T(128)}, f32[256,256]{1,0:T(8,128)S(1)}, bf16[8,256,256]{2,1,0:T(8,128)(2,1)}, f32[8]{0:T(128)S(1)}, ...), condition=%wide.region_3.3_spmd.clone, body=%wide.region_2.2_spmd.clone.sunk | while | flops 262147 | bytes 1180268 | solution.py:70
  126.4 0.9 copy-done
  127.5 0.7 bitcast_dynamic-update-slice_fusion.9
  128.2 1.1 bitcast_convert_fusion.3
  129.4 1.2 fusion.71
  130.5 0.7 dynamic-slice_reduce_fusion.2
  131.8 1.0 constant_dynamic-slice_fusion.2
  132.8 0.7 fusion.74
  133.6 15.8 %while.31 = (s32[]{:T(128)}, f32[256,256]{1,0:T(8,128)S(1)}, bf16[8,256,256]{2,1,0:T(8,128)(2,1)}, f32[8]{0:T(128)S(1)}, f32[8,256,256]{2,1,0:T(8,128)S(1)}, /*index=5*/s32[]{:T(128)}, s32[]{:T(128)}) while((s32[]{:T(128)}, f32[256,256]{1,0:T(8,128)S(1)}, bf16[8,256,256]{2,1,0:T(8,128)(2,1)}, f32[8]{0:T(128)S(1)}, ...), condition=%wide.region_3.3_spmd.clone, body=%wide.region_2.2_spmd.clone.sunk | while | flops 262147 | bytes 1180268 | solution.py:70
  148.7 0.7 bitcast_add_fusion.2
  149.7 0.9 copy-done
  150.9 0.7 bitcast_dynamic-update-slice_fusion.9
  151.6 1.1 bitcast_convert_fusion.3
  152.7 1.2 fusion.71
  153.9 0.7 dynamic-slice_reduce_fusion.2
  155.2 1.0 constant_dynamic-slice_fusion.2
  156.2 0.7 fusion.74
  156.9 15.8 %while.31 = (s32[]{:T(128)}, f32[256,256]{1,0:T(8,128)S(1)}, bf16[8,256,256]{2,1,0:T(8,128)(2,1)}, f32[8]{0:T(128)S(1)}, f32[8,256,256]{2,1,0:T(8,128)S(1)}, /*index=5*/s32[]{:T(128)}, s32[]{:T(128)}) while((s32[]{:T(128)}, f32[256,256]{1,0:T(8,128)S(1)}, bf16[8,256,256]{2,1,0:T(8,128)(2,1)}, f32[8]{0:T(128)S(1)}, ...), condition=%wide.region_3.3_spmd.clone, body=%wide.region_2.2_spmd.clone.sunk | while | flops 262147 | bytes 1180268 | solution.py:70
  164.1 0.7 bitcast_add_fusion.2
  172.0 0.7 bitcast_add_fusion.2
  173.1 0.9 copy-done
  174.3 0.7 bitcast_dynamic-update-slice_fusion.9
  175.0 2.0 copy.29
  177.0 37.4 %all_to_all.45 = bf16[4,512,256]{2,0,1:T(4,128)(2,1)S(1)} all-to-all(bf16[4,512,256]{2,0,1:T(4,128)(2,1)S(1)} %copy.29), channel_id=1, replica_groups=mesh['sp'=8,'dp'=4] {'sp'}, dimensions={1} | all-to-all | bytes 2097152 | tf_op jit(solution)/shard_map/all_to_all | solution.py:101
  215.9 6.7 %fusion.48 = bf16[4,64,2048]{2,1,0:T(8,128)(2,1)} fusion(bf16[8,256,2048]{2,1,0:T(8,128)(2,1)} %all-gather.2.cloned.1.call-done, f32[4,8,64]{2,1,0:T(8,128)S(1)} %bitcast.139, f32[4,8,64,256]{3,2,1,0:T(8,128)S(1)} %bitcast.135), kind=kOutput, calls=%fused_computation.60 | convolution fusion | flops 2149056512 | bytes 11542528 | tf_op jit(solution)/shard_map/shtd,hde->ste/dot_general | solution.py:107
  (156 shorter events, 66.7 us)
Async XLA Ops:
  6.5 7.5 %copy-start.1 = (bf16[4,8,64,256]{3,2,1,0:T(8,128)(2,1)S(1)}, bf16[4,8,64,256]{3,2,1,0:T(8,128)(2,1)}, u32[]{:S(2)}) copy-start(bf16[4,8,64,256]{3,2,1,0:T(8,128)(2,1)} %param.11) | copy-start | bytes 3145732
  6.5 40.2 %all-to-all-start = ((bf16[32,64,256]{2,1,0:T(8,128)(2,1)}), bf16[32,64,256]{2,1,0:T(8,128)(2,1)S(1)}, u32[]{:S(2)}, u32[]{:S(2)}) async-start(bf16[32,64,256]{2,1,0:T(8,128)(2,1)} %bitcast.137), calls=%async_computation | async-start | bytes 2097152 | tf_op jit(solution)/shard_map/all_to_all | solution.py:89
  13.9 201.9 %all-gather.2.cloned.1.call-start = ((), (), s32[]{:S(2)}) async-start(), calls=%async_computation.3 | async-start | bytes 10485760 | tf_op jit(solution)/shard_map/all_gather | solution.py:110
  14.8 35.5 %collective-permute-start = (bf16[4,64,256]{2,1,0:T(8,128)(2,1)S(1)}, bf16[4,64,256]{2,1,0:T(8,128)(2,1)}, u32[]{:S(2)}, u32[]{:S(2)}) collective-permute-start(bf16[4,64,256]{2,1,0:T(8,128)(2,1)S(1)} %get-tuple-element.226), channel_id=1, source_target_pairs={{0,4},{4,0},{8,12},{12,8},{16,20},{20,16},{24,28},{28,24},{1,5},{5... | collective-permute-start | bytes 393224 | tf_op jit(solution)/shard_map/ppermute | solution.py:27
  16.8 38.9 %collective-permute-start.1 = (bf16[4,64,256]{2,1,0:T(8,128)(2,1)S(1)}, bf16[4,64,256]{2,1,0:T(8,128)(2,1)S(1)}, u32[]{:S(2)}, u32[]{:S(2)}) collective-permute-start(bf16[4,64,256]{2,1,0:T(8,128)(2,1)S(1)} %get-tuple-element.225), channel_id=1, source_target_pairs={{0,8},{4,12},{8,0},{12,4},{16,24},{20,28},{24,16},{28,20},{1,9},{5... | collective-permute-start | bytes 393224 | tf_op jit(solution)/shard_map/ppermute | solution.py:27
  18.2 39.6 %collective-permute-start.2 = (bf16[4,64,256]{2,1,0:T(8,128)(2,1)S(1)}, bf16[4,64,256]{2,1,0:T(8,128)(2,1)S(1)}, u32[]{:S(2)}, u32[]{:S(2)}) collective-permute-start(bf16[4,64,256]{2,1,0:T(8,128)(2,1)S(1)} %get-tuple-element.224), channel_id=1, source_target_pairs={{0,12},{4,8},{8,4},{12,0},{16,28},{20,24},{24,20},{28,16},{1,13},{... | collective-permute-start | bytes 393224 | tf_op jit(solution)/shard_map/ppermute | solution.py:27
  18.3 40.1 %collective-permute-start.3 = (bf16[4,64,256]{2,1,0:T(8,128)(2,1)S(1)}, bf16[4,64,256]{2,1,0:T(8,128)(2,1)S(1)}, u32[]{:S(2)}, u32[]{:S(2)}) collective-permute-start(bf16[4,64,256]{2,1,0:T(8,128)(2,1)S(1)} %get-tuple-element.223), channel_id=1, source_target_pairs={{0,16},{4,20},{8,24},{12,28},{16,0},{20,4},{24,8},{28,12},{1,17},{... | collective-permute-start | bytes 393224 | tf_op jit(solution)/shard_map/ppermute | solution.py:27
  21.2 38.6 %collective-permute-start.4 = (bf16[4,64,256]{2,1,0:T(8,128)(2,1)S(1)}, bf16[4,64,256]{2,1,0:T(8,128)(2,1)S(1)}, u32[]{:S(2)}, u32[]{:S(2)}) collective-permute-start(bf16[4,64,256]{2,1,0:T(8,128)(2,1)S(1)} %get-tuple-element.222), channel_id=1, source_target_pairs={{0,20},{4,16},{8,28},{12,24},{16,4},{20,0},{24,12},{28,8},{1,21},{... | collective-permute-start | bytes 393224 | tf_op jit(solution)/shard_map/ppermute | solution.py:27
  46.7 33.8 %all-to-all-start.1 = ((bf16[32,64,256]{2,1,0:T(8,128)(2,1)}), bf16[32,64,256]{2,1,0:T(8,128)(2,1)S(1)}, u32[]{:S(2)}, u32[]{:S(2)}) async-start(bf16[32,64,256]{2,1,0:T(8,128)(2,1)} %bitcast.4), calls=%async_computation.1 | async-start | bytes 2097152 | tf_op jit(solution)/shard_map/all_to_all | solution.py:86
  50.3 19.8 %collective-permute-start.5 = (bf16[4,64,256]{2,1,0:T(8,128)(2,1)S(1)}, bf16[4,64,256]{2,1,0:T(8,128)(2,1)S(1)}, u32[]{:S(2)}, u32[]{:S(2)}) collective-permute-start(bf16[4,64,256]{2,1,0:T(8,128)(2,1)S(1)} %get-tuple-element.221), channel_id=1, source_target_pairs={{0,24},{4,28},{8,16},{12,20},{16,8},{20,12},{24,0},{28,4},{1,25},{... | collective-permute-start | bytes 393224 | tf_op jit(solution)/shard_map/ppermute | solution.py:27
  55.7 16.9 %collective-permute-start.6 = (bf16[4,64,256]{2,1,0:T(8,128)(2,1)S(1)}, bf16[4,64,256]{2,1,0:T(8,128)(2,1)S(1)}, u32[]{:S(2)}, u32[]{:S(2)}) collective-permute-start(bf16[4,64,256]{2,1,0:T(8,128)(2,1)S(1)} %get-tuple-element.220), channel_id=1, source_target_pairs={{0,28},{4,24},{8,20},{12,16},{16,12},{20,8},{24,4},{28,0},{1,29},{... | collective-permute-start | bytes 393224 | tf_op jit(solution)/shard_map/ppermute | solution.py:27
  102.6 1.2 copy-start
  126.0 1.2 copy-start
  149.4 1.2 copy-start
  172.7 1.2 copy-start
Sparse Core Ops, SparseCore 0:
  22.8 58.2 all-gather.1
